TPU v7x, 32 devices: a whole 2x2x4 slice. The times are simulated.
32 devices in a mesh: grp: 2 (over y), fs: 4 (over z), tp: 4 (over x, core).
Axes of the slice: x: 2, y: 2, z: 4, core: 2. Of those that a mesh axis runs over, the one named last changes fastest.
Arguments:
- tokens: bfloat16 [6144, 2048], P(('grp', 'fs')), parts along dimension 0, may hold values from -6 to 6
- pre_gain: float32 [2048], replicated, may hold values from 0.1 to 1.9
- up_weight: bfloat16 [2048, 8192], P('fs', 'tp'), may hold values from -0.125 to 0.125
- down_weight: bfloat16 [8192, 2048], P(('tp', 'fs')), as said below
- post_gain: float32 [2048], P('tp'), may hold values from 0.1 to 1.9
Outputs:
- mixed: bfloat16 [6144, 2048], P(('grp', 'fs'), 'tp'), parts along dimension 0
There are 2 independent parts, one for each index of `grp`. A program takes and returns all parts, laid end to end along the dimension named above; an argument that names none is the same for every part. Nothing has to cross between parts.
Inputs may be any that keep to these rules, and one draw needn't show every extreme that they name: `down_weight`: a matrix whose columns fall into 4 consecutive blocks of different magnitudes.
All inputs are finite; a program needn't handle non-finite values.
Results may differ from a plain program's by a relative error of at most 0.014.
Values may be sent and summed in bfloat16 or wider, within the bound.
A program may use at most 64 MiB of HBM per device.

v0:
```python
import jax
import jax.numpy as jnp
from jax import lax
from jax.sharding import PartitionSpec as P


def shards(tokens, pre_gain, up_weight, down_weight, post_gain):
    eps = 1e-06
    values = tokens.astype(jnp.float32)
    normed = (
        values * lax.rsqrt(jnp.mean(values * values, axis=1, keepdims=True) + eps) * pre_gain
    ).astype(jnp.bfloat16)
    full_up = lax.all_gather(up_weight, "fs", axis=0, tiled=True)
    up = jnp.dot(normed, full_up, preferred_element_type=jnp.float32)
    hidden = jnp.square(jnp.maximum(up, 0.0)).astype(jnp.bfloat16)
    full_down = lax.all_gather(down_weight, "fs", axis=0, tiled=True)
    partial_terms = jnp.dot(hidden, full_down, preferred_element_type=jnp.float32)
    own_width = post_gain.shape[0]
    full_width = lax.axis_size("tp") * own_width
    mixed = lax.psum_scatter(
        partial_terms.astype(jnp.bfloat16), "tp", scatter_dimension=1, tiled=True
    ).astype(jnp.float32)
    squares = lax.psum(jnp.sum(mixed * mixed, axis=1), "tp")
    factor = lax.rsqrt(squares / full_width + eps)
    return (mixed * factor[:, None] * post_gain).astype(jnp.bfloat16)


def solution(mesh):
    in_specs = (P(("grp", "fs"), None), P(), P("fs", "tp"), P(("tp", "fs"), None), P("tp"))
    out_specs = P(("grp", "fs"), "tp")
    return jax.shard_map(shards, mesh=mesh, in_specs=in_specs, out_specs=out_specs, check_vma=False)
```

profile of v0, /device:TPU:0, one launch (start us, length us, event | category | flops | bytes accessed | tf_op | source)
XLA Modules:
  0.0 383.3 jit_solution(18431239371068029638)
XLA Ops:
  6.5 0.0 copy-start
  6.5 0.0 copy-start.2
  6.5 0.0 all-gather.3.cloned.1.call-start
  6.5 0.7 all-gather.3.cloned.1.call-update
  7.3 0.0 all-gather.5.cloned.1.call-start
  7.3 0.7 all-gather.5.cloned.1.call-update
  8.0 0.0 reduce-scatter.2.cloned.1.call-start
  8.1 0.4 copy-done
  8.4 0.7 fusion
  9.1 0.0 copy-start.1
  9.1 152.1 %all-gather.3.cloned.1.call-done = bf16[2048,2048]{1,0:T(8,128)(2,1)} async-done(((bf16[512,2048]{1,0:T(8,128)(2,1)}), bf16[2048,2048]{1,0:T(8,128)(2,1)}) %all-gather.3.cloned.1.call-update) | async-done | bytes 8388624 | tf_op jit(solution)/shard_map/all_gather | solution.py:13
  161.3 149.4 %all-gather.5.cloned.1.call-done = bf16[2048,2048]{1,0:T(8,128)(2,1)} async-done(((bf16[512,2048]{1,0:T(8,128)(2,1)}), bf16[2048,2048]{1,0:T(8,128)(2,1)}) %all-gather.5.cloned.1.call-update) | async-done | bytes 8388624 | tf_op jit(solution)/shard_map/all_gather | solution.py:16
  310.7 0.0 copy-done.2
  310.7 20.6 %convolution_convert_fusion = bf16[768,2048]{1,0:T(8,128)(2,1)} fusion(bf16[2048,2048]{1,0:T(8,128)(2,1)} %all-gather.5.cloned.1.call-done, bf16[2048,2048]{1,0:T(8,128)(2,1)} %all-gather.3.cloned.1.call-done, bf16[768,2048]{1,0:T(8,128)(2,1)S(1)} %copy-done, f32[2048]{0:T(1024)S(1)} %copy-done.2, f32[768]{0:T(1024)S(1)} %add_rsqrt_fusion.1), kind=kOutput, calls=%fused_computation.6 | convolution fusion | flops 12897484800 | bytes 23079936 | tf_op jit(solution)/shard_map/dot_general | solution.py:17
  331.3 0.0 reduce-scatter.2.cloned.1.call-update
  331.3 36.1 %reduce-scatter.2.cloned.1.call-done = bf16[768,512]{1,0:T(8,128)(2,1)} async-done(((bf16[768,2048]{1,0:T(8,128)(2,1)}), bf16[768,512]{1,0:T(8,128)(2,1)}) %reduce-scatter.2.cloned.1.call-update) | async-done | bytes 786448 | tf_op jit(solution)/shard_map/reduce_scatter | solution.py:20
  367.4 1.4 fusion.6
  368.7 5.8 %psum.7 = f32[768]{0:T(1024)S(1)} all-reduce(f32[768]{0:T(1024)S(1)} %fusion.6), channel_id=1, replica_groups=mesh['grp'=2,'fs'=4,'tp'=4] {'tp'}, use_global_device_ids=true, to_apply=%region_3.0 | all-reduce | flops 768 | bytes 6144 | tf_op jit(solution)/shard_map/psum | solution.py:23
  374.5 0.0 copy-done.1
  374.5 2.3 fusion.8
  (2 shorter events, 0.0 us)
Async XLA Ops:
  6.5 1.9 copy-start
  6.5 304.1 %copy-start.2 = (f32[2048]{0:T(1024)S(1)}, f32[2048]{0:T(1024)}, u32[]{:S(2)}) copy-start(f32[2048]{0:T(1024)} %param.6) | copy-start | bytes 24580
  6.5 154.7 %all-gather.3.cloned.1.call-start = ((), (), s32[]{:S(2)}) async-start(), calls=%async_computation.1 | async-start | bytes 10485760 | tf_op jit(solution)/shard_map/all_gather | solution.py:13
  7.3 303.4 %all-gather.5.cloned.1.call-start = ((), (), s32[]{:S(2)}) async-start(), calls=%async_computation.2 | async-start | bytes 10485760 | tf_op jit(solution)/shard_map/all_gather | solution.py:16
  8.0 359.3 %reduce-scatter.2.cloned.1.call-start = ((), (), s32[]{:S(2)}) async-start(), calls=%async_computation.3 | async-start | bytes 3932160 | tf_op jit(solution)/shard_map/reduce_scatter | solution.py:20
  9.1 365.4 %copy-start.1 = (f32[512]{0:T(512)S(1)}, f32[512]{0:T(512)}, u32[]{:S(2)}) copy-start(f32[512]{0:T(512)} %param.9) | copy-start | bytes 6148
Sparse Core Ops, SparseCore 0:
  8.9 152.3 all-gather.2
  162.8 147.7 all-gather.4
  331.4 35.8 reduce-scatter.1
where the time goes:
time: 383 us
  waiting for transfers between devices  339 us (89%)
  matrix products  20.6 us (5%)
  between operations  13.1 us (3%)
  blocking collectives  5.77 us (2%)
  other arithmetic  4.31 us (1%)
    all_gather x1, waiting for transfers between devices, shards(): full_up = lax.all_gather(up_weight, 'fs', axis=0, tiled=True)  152 us
    all_gather x1, waiting for transfers between devices, shards(): full_down = lax.all_gather(down_weight, 'fs', axis=0, tiled=True)  149 us
    reduce_scatter x1, waiting for transfers between devices, shards(): lax.psum_scatter(partial_terms.astype(jnp.bfloat16), 'tp', scatter_dimens...  36.1 us
    dot_general x1, matrix products, shards(): jnp.dot(hidden, full_down, preferred_element_type=jnp.float32)  20.6 us
  transfers between devices with their start and end apart: 3, of which 3 were waited for; matrix products, arithmetic and copies ran while one was open for 0% of the time, Pallas kernels for 0%

commit v1 on v0

--- a/solution.py
+++ b/solution.py
@@ -2,6 +2,16 @@
 import jax.numpy as jnp
 from jax import lax
 from jax.sharding import PartitionSpec as P
+
+
+def around_the_ring(shard, name, dim):
+    size = lax.axis_size(name)
+    held, parts = (shard, [shard])
+    for _ in range(size - 1):
+        held = lax.ppermute(held, name, [(i, (i + 1) % size) for i in range(size)])
+        parts.insert(0, held)
+    line = jnp.concatenate(parts, axis=dim)
+    return jnp.roll(line, (lax.axis_index(name) + 1) * shard.shape[dim], axis=dim)
 
 
 def shards(tokens, pre_gain, up_weight, down_weight, post_gain):
@@ -10,7 +20,7 @@
     normed = (
         values * lax.rsqrt(jnp.mean(values * values, axis=1, keepdims=True) + eps) * pre_gain
     ).astype(jnp.bfloat16)
-    full_up = lax.all_gather(up_weight, "fs", axis=0, tiled=True)
+    full_up = around_the_ring(up_weight, "fs", 0)
     up = jnp.dot(normed, full_up, preferred_element_type=jnp.float32)
     hidden = jnp.square(jnp.maximum(up, 0.0)).astype(jnp.bfloat16)
     full_down = lax.all_gather(down_weight, "fs", axis=0, tiled=True)

time: 383 us -> 364 us (0.950)
  waiting for transfers between devices: 339 us -> 259 us
  starting transfers between devices: 0.08 us -> 54.2 us
  local copies, waits for them, and re-layouts: 0.38 us -> 8.07 us
    ppermute x0 -> x3, waiting for transfers between devices: none -> 221 us  [around_the_ring(): held = lax.ppermute(held, name, [(i, (i + 1) % size) for i in range(size)])]
    all_gather x1 -> x0, waiting for transfers between devices: 152 us -> none  [shards(): full_up = lax.all_gather(up_weight, 'fs', axis=0, tiled=True)]
    all_gather x1, waiting for transfers between devices: 149 us -> 0.02 us  [shards(): full_down = lax.all_gather(down_weight, 'fs', axis=0, tiled=True)]
    ppermute x0 -> x3, starting transfers between devices: none -> 54.2 us  [around_the_ring(): held = lax.ppermute(held, name, [(i, (i + 1) % size) for i in range(size)])]
    dot_general x1, matrix products: 20.6 us -> 10.3 us  [shards(): jnp.dot(hidden, full_down, preferred_element_type=jnp.float32)]
    unnamed x6 -> x15, local copies, waits for them, and re-layouts: 0.38 us -> 7.83 us
    dot_general x0 -> x1, matrix products: none -> 7.05 us  [shards(): up = jnp.dot(normed, full_up, preferred_element_type=jnp.float32)]
  transfers between devices with their start and end apart: 3 -> 5, of which waited for: 3 -> 4; matrix products, arithmetic and copies ran while one was open for 0% -> 5% of each run, Pallas kernels for 0% -> 0%
where the time goes in v1:
time: 364 us
  waiting for transfers between devices  259 us (71%)
  starting transfers between devices  54.2 us (15%)
  matrix products  17.4 us (5%)
  between operations  13.5 us (4%)
  local copies, waits for them, and re-layouts  8.07 us (2%)
  other arithmetic  6.2 us (2%)
  blocking collectives  5.77 us (2%)
    ppermute x3, waiting for transfers between devices, around_the_ring(): held = lax.ppermute(held, name, [(i, (i + 1) % size) for i in range(size)])  221 us
    ppermute x3, starting transfers between devices, around_the_ring(): held = lax.ppermute(held, name, [(i, (i + 1) % size) for i in range(size)])  54.2 us
    reduce_scatter x1, waiting for transfers between devices, shards(): lax.psum_scatter(partial_terms.astype(jnp.bfloat16), 'tp', scatter_dimens...  37.2 us
    dot_general x1, matrix products, shards(): jnp.dot(hidden, full_down, preferred_element_type=jnp.float32)  10.3 us
    unnamed x15, local copies, waits for them, and re-layouts  7.83 us
  transfers between devices with their start and end apart: 5, of which 4 were waited for; matrix products, arithmetic and copies ran while one was open for 5% of the time, Pallas kernels for 0%

profile of v1, /device:TPU:0, one launch (start us, length us, event | category | flops | bytes accessed | tf_op | source)
XLA Modules:
  0.0 363.7 jit_solution(4662282292436579426)
XLA Ops:
  6.5 0.7 all-gather.2.cloned.1.call-update
  7.3 0.0 reduce-scatter.2.cloned.1.call-start
  7.3 3.1 collective-permute-start
  10.4 81.4 %collective-permute-done = bf16[512,2048]{1,0:T(8,128)(2,1)S(1)} collective-permute-done((bf16[512,2048]{1,0:T(8,128)(2,1)}, bf16[512,2048]{1,0:T(8,128)(2,1)S(1)}, u32[]{:S(2)}, u32[]{:S(2)}) %collective-permute-start) | collective-permute-done | bytes 2097184 | tf_op jit(solution)/shard_map/ppermute | solution.py:11
  91.8 33.4 %collective-permute-start.1 = (bf16[512,2048]{1,0:T(8,128)(2,1)S(1)}, bf16[512,2048]{1,0:T(8,128)(2,1)}, u32[]{:S(2)}, u32[]{:S(2)}) collective-permute-start(bf16[512,2048]{1,0:T(8,128)(2,1)S(1)} %collective-permute-done), channel_id=1, source_target_pairs={{0,4},{4,8},{8,12},{12,0},{1,5},{5,9},{9,13},{13,1},{2,6},{6,10},{... | collective-permute-start | bytes 6291464 | tf_op jit(solution)/shard_map/ppermute | solution.py:11
  125.2 93.9 %collective-permute-done.1 = bf16[512,2048]{1,0:T(8,128)(2,1)} collective-permute-done((bf16[512,2048]{1,0:T(8,128)(2,1)S(1)}, bf16[512,2048]{1,0:T(8,128)(2,1)}, u32[]{:S(2)}, u32[]{:S(2)}) %collective-permute-start.1) | collective-permute-done | bytes 2097184 | tf_op jit(solution)/shard_map/ppermute | solution.py:11
  219.1 17.7 %collective-permute-start.2 = (bf16[512,2048]{1,0:T(8,128)(2,1)}, bf16[512,2048]{1,0:T(8,128)(2,1)}, u32[]{:S(2)}, u32[]{:S(2)}) collective-permute-start(bf16[512,2048]{1,0:T(8,128)(2,1)} %collective-permute-done.1), channel_id=1, source_target_pairs={{0,4},{4,8},{8,12},{12,0},{1,5},{5,9},{9,13},{13,1},{2,6},{6,10},{... | collective-permute-start | bytes 6291464 | tf_op jit(solution)/shard_map/ppermute | solution.py:11
  236.8 2.6 fusion.2
  239.4 45.2 %collective-permute-done.2 = bf16[512,2048]{1,0:T(8,128)(2,1)} collective-permute-done((bf16[512,2048]{1,0:T(8,128)(2,1)}, bf16[512,2048]{1,0:T(8,128)(2,1)}, u32[]{:S(2)}, u32[]{:S(2)}) %collective-permute-start.2) | collective-permute-done | bytes 2097184 | tf_op jit(solution)/shard_map/ppermute | solution.py:11
  284.6 1.7 constant_dynamic-update-slice_fusion.7
  286.4 1.7 constant_dynamic-update-slice_fusion.6
  288.1 0.1 constant_dynamic-update-slice_fusion.5
  288.2 0.2 constant_dynamic-update-slice_fusion.4
  288.5 1.7 constant_dynamic-update-slice_fusion.3
  290.2 1.9 constant_dynamic-update-slice_fusion.2
  292.1 0.1 constant_dynamic-update-slice_fusion.1
  292.3 0.2 constant_dynamic-update-slice_fusion
  292.5 0.2 copy-done.1
  292.8 7.1 %multiply_convert_fusion = bf16[768,2048]{1,0:T(8,128)(2,1)S(1)} fusion(bf16[4096,2048]{1,0:T(8,128)(2,1)S(1)} %constant_dynamic-update-slice_fusion, s32[]{:T(128)S(6)} %select_n.14, bf16[768,2048]{1,0:T(8,128)(2,1)S(1)} %copy-done.1, f32[2048]{0:T(1024)S(1)} %copy-done.3, f32[768]{0:T(1024)S(1)} %add_rsqrt_fusion.1), kind=kOutput, calls=%fused_computation.7 | convolution fusion | flops 6453460992 | bytes 14692356 | tf_op jit(solution)/shard_map/dot_general | solution.py:24
  299.9 10.3 %convolution_convert_fusion = bf16[768,2048]{1,0:T(8,128)(2,1)} fusion(bf16[768,2048]{1,0:T(8,128)(2,1)S(1)} %multiply_convert_fusion, bf16[2048,2048]{1,0:T(8,128)(2,1)} %all-gather.2.cloned.1.call-done), kind=kOutput, calls=%fused_computation.8 | convolution fusion | flops 6444023808 | bytes 14680064 | tf_op jit(solution)/shard_map/dot_general | solution.py:27
  310.2 37.2 %reduce-scatter.2.cloned.1.call-done = bf16[768,512]{1,0:T(8,128)(2,1)} async-done(((bf16[768,2048]{1,0:T(8,128)(2,1)}), bf16[768,512]{1,0:T(8,128)(2,1)}) %reduce-scatter.2.cloned.1.call-update) | async-done | bytes 786448 | tf_op jit(solution)/shard_map/reduce_scatter | solution.py:30
  347.4 1.4 fusion.10
  348.8 5.8 %psum.7 = f32[768]{0:T(1024)S(1)} all-reduce(f32[768]{0:T(1024)S(1)} %fusion.10), channel_id=1, replica_groups=mesh['grp'=2,'fs'=4,'tp'=4] {'tp'}, use_global_device_ids=true, to_apply=%region_3.4 | all-reduce | flops 768 | bytes 6144 | tf_op jit(solution)/shard_map/psum | solution.py:33
  354.6 2.3 fusion.12
  (12 shorter events, 0.1 us)
Async XLA Ops:
  6.5 293.3 %all-gather.2.cloned.1.call-start = ((), (), s32[]{:S(2)}) async-start(), calls=%async_computation.1 | async-start | bytes 10485760 | tf_op jit(solution)/shard_map/all_gather | solution.py:26
  7.3 340.2 %reduce-scatter.2.cloned.1.call-start = ((), (), s32[]{:S(2)}) async-start(), calls=%async_computation.2 | async-start | bytes 3932160 | tf_op jit(solution)/shard_map/reduce_scatter | solution.py:30
  7.3 84.5 %collective-permute-start = (bf16[512,2048]{1,0:T(8,128)(2,1)}, bf16[512,2048]{1,0:T(8,128)(2,1)S(1)}, u32[]{:S(2)}, u32[]{:S(2)}) collective-permute-start(bf16[512,2048]{1,0:T(8,128)(2,1)} %param.7), channel_id=1, source_target_pairs={{0,4},{4,8},{8,12},{12,0},{1,5},{5,9},{9,13},{13,1},{2,6},{6,10},{... | collective-permute-start | bytes 6291464 | tf_op jit(solution)/shard_map/ppermute | solution.py:11
  91.8 127.3 %collective-permute-start.1 = (bf16[512,2048]{1,0:T(8,128)(2,1)S(1)}, bf16[512,2048]{1,0:T(8,128)(2,1)}, u32[]{:S(2)}, u32[]{:S(2)}) collective-permute-start(bf16[512,2048]{1,0:T(8,128)(2,1)S(1)} %collective-permute-done), channel_id=1, source_target_pairs={{0,4},{4,8},{8,12},{12,0},{1,5},{5,9},{9,13},{13,1},{2,6},{6,10},{... | collective-permute-start | bytes 6291464 | tf_op jit(solution)/shard_map/ppermute | solution.py:11
  219.1 65.5 %collective-permute-start.2 = (bf16[512,2048]{1,0:T(8,128)(2,1)}, bf16[512,2048]{1,0:T(8,128)(2,1)}, u32[]{:S(2)}, u32[]{:S(2)}) collective-permute-start(bf16[512,2048]{1,0:T(8,128)(2,1)} %collective-permute-done.1), channel_id=1, source_target_pairs={{0,4},{4,8},{8,12},{12,0},{1,5},{5,9},{9,13},{13,1},{2,6},{6,10},{... | collective-permute-start | bytes 6291464 | tf_op jit(solution)/shard_map/ppermute | solution.py:11
  239.4 48.8 %copy-start = (bf16[512,2048]{1,0:T(8,128)(2,1)S(1)}, bf16[512,2048]{1,0:T(8,128)(2,1)}, u32[]{:S(2)}) copy-start(bf16[512,2048]{1,0:T(8,128)(2,1)} %param.7) | copy-start | bytes 6291460
  290.2 2.5 copy-start.1
  290.2 2.5 copy-start.3
  299.8 54.7 %copy-start.2 = (f32[512]{0:T(512)S(1)}, f32[512]{0:T(512)}, u32[]{:S(2)}) copy-start(f32[512]{0:T(512)} %param.9) | copy-start | bytes 6148
Sparse Core Ops, SparseCore 0:
  8.9 229.6 all-gather.1
  310.3 37.0 reduce-scatter.1
